TPU v7x, 32 devices: a whole 2x2x4 slice. The times are simulated.
32 devices in a mesh: ra: 8 (over z, x), cb: 4 (over y, core).
Axes of the slice: x: 2, y: 2, z: 4, core: 2. Of those that a mesh axis runs over, the one named last changes fastest.
Arguments:
- tokens: bfloat16 [64, 1024], P(None, 'ra'), may hold values from -14 to 14, as said below
- norm_gain_a: float32 [1024], P('ra'), may hold values from 0.1 to 1.9
- gate_weight_a: float32 [1024, 2816], P('ra', 'cb'), may hold values from -0.1875 to 0.1875
- up_weight_a: float32 [1024, 2816], P('ra', 'cb'), may hold values from -0.1875 to 0.1875
- down_weight_a: float32 [2816, 1024], P('cb', 'ra'), may hold values from -0.109375 to 0.109375
- norm_gain_b: float32 [1024], P('ra'), may hold values from 0.1 to 1.9
- gate_weight_b: float32 [1024, 2816], P('ra', 'cb'), may hold values from -0.1875 to 0.1875
- up_weight_b: float32 [1024, 2816], P('ra', 'cb'), may hold values from -0.1875 to 0.1875
- down_weight_b: float32 [2816, 1024], P('cb', 'ra'), may hold values from -0.109375 to 0.109375
Outputs:
- stream_out: bfloat16 [64, 1024], P(None, 'ra')
Inputs may be any that keep to these rules, and one draw needn't show every extreme that they name: Each feature of tokens carries its own scale, between about 0.3 and 3.3 across features; entries lie within -14 to 14.
All inputs are finite; a program needn't handle non-finite values.
Results may differ from a plain program's by a relative error of at most 0.008.
Values may be sent and summed in bfloat16 or wider, within the bound.
A program may use at most 64 MiB of HBM per device.

v0:
```python
import jax
import jax.numpy as jnp
from jax import lax
from jax.sharding import PartitionSpec as P

residual_weight = 0.5
epsilon = 1e-06


def hidden_of(normed, gate_cast, up_cast):
    gate_part = jnp.dot(normed, gate_cast, preferred_element_type=jnp.float32)
    up_part = jnp.dot(normed, up_cast, preferred_element_type=jnp.float32)
    gate_sum, up_sum = lax.psum((gate_part, up_part), "ra")
    return (jax.nn.silu(gate_sum) * up_sum).astype(jnp.bfloat16)


def normalize(as_float, square_total, gain):
    feature_count = as_float.shape[1] * lax.axis_size("ra")
    row_scale = lax.rsqrt(square_total / feature_count + epsilon)
    return (as_float * row_scale[:, None] * gain).astype(jnp.bfloat16)


def whole_sublayer(stream, gain, gate_weight, up_weight, down_weight):
    as_float = stream.astype(jnp.float32)
    square_total = lax.psum(jnp.sum(as_float * as_float, axis=1), "ra")
    normed = normalize(as_float, square_total, gain)
    hidden = hidden_of(normed, gate_weight.astype(jnp.bfloat16), up_weight.astype(jnp.bfloat16))
    branch_part = jnp.dot(
        hidden, down_weight.astype(jnp.bfloat16), preferred_element_type=jnp.float32
    )
    branch = lax.psum(branch_part, "cb")
    return (residual_weight * as_float + branch).astype(jnp.bfloat16)


def per_device(
    tokens,
    norm_gain_a,
    gate_weight_a,
    up_weight_a,
    down_weight_a,
    norm_gain_b,
    gate_weight_b,
    up_weight_b,
    down_weight_b,
):
    middle = whole_sublayer(tokens, norm_gain_a, gate_weight_a, up_weight_a, down_weight_a)
    return whole_sublayer(middle, norm_gain_b, gate_weight_b, up_weight_b, down_weight_b)


def solution(mesh):
    placed = (
        P(None, "ra"),
        P("ra"),
        P("ra", "cb"),
        P("ra", "cb"),
        P("cb", "ra"),
        P("ra"),
        P("ra", "cb"),
        P("ra", "cb"),
        P("cb", "ra"),
    )
    return jax.shard_map(
        per_device, mesh=mesh, in_specs=placed, out_specs=P(None, "ra"), check_vma=False
    )
```

profile of v0, /device:TPU:0, one launch (start us, length us, event | category | flops | bytes accessed | tf_op | source)
XLA Modules:
  0.0 224.6 jit_solution(7267552355934892765)
XLA Ops:
  6.5 0.0 all-reduce.7.cloned.1.call-start
  6.5 0.9 fusion.14
  7.4 23.1 %psum.56 = f32[64]{0:T(128)S(1)} all-reduce(f32[64]{0:T(128)S(1)} %fusion.14), channel_id=1, replica_groups=mesh['ra'=8,'cb'=4] {'ra'}, use_global_device_ids=true, to_apply=%region_1.0 | all-reduce | flops 64 | bytes 512 | tf_op jit(solution)/shard_map/psum | solution.py:25
  30.6 0.0 copy-done.3
  30.6 0.0 copy-start.4
  30.6 1.9 fusion.8
  32.5 0.0 copy-done
  32.5 0.0 copy-done.4
  32.5 0.9 fusion.10
  33.4 0.0 all-reduce.7.cloned.1.call-update
  33.5 0.0 all-reduce.5.cloned.1.call-start
  33.5 69.4 %all-reduce.7.cloned.1.call-done = (f32[64,704]{1,0:T(8,128)}, f32[64,704]{1,0:T(8,128)}) async-done(((f32[64,704]{1,0:T(8,128)}, f32[64,704]{1,0:T(8,128)}), (f32[64,704]{1,0:T(8,128)}, f32[64,704]{1,0:T(8,128)})) %all-reduce.7.cloned.1.call-update) | async-done | bytes 360464 | tf_op jit(solution)/shard_map/psum | solution.py:13
  102.9 1.3 fusion.6
  104.1 0.0 copy-start.2
  104.2 10.4 %psum.59 = f32[64,128]{1,0:T(8,128)S(1)} all-reduce(f32[64,128]{1,0:T(8,128)S(1)} %fusion.6), channel_id=1, replica_groups=mesh['ra'=8,'cb'=4] {'cb'}, use_global_device_ids=true, to_apply=%region_4.5 | all-reduce | flops 8192 | bytes 65536 | tf_op jit(solution)/shard_map/psum | solution.py:31
  114.6 0.1 fusion.19
  114.7 19.5 %psum.60 = f32[64]{0:T(128)S(1)} all-reduce(f32[64]{0:T(128)S(1)} %get-tuple-element.9), channel_id=1, replica_groups=mesh['ra'=8,'cb'=4] {'ra'}, use_global_device_ids=true, to_apply=%region_6.7 | all-reduce | flops 64 | bytes 512 | tf_op jit(solution)/shard_map/psum | solution.py:25
  134.2 0.9 fusion.2
  135.1 0.9 fusion.4
  136.1 0.0 all-reduce.5.cloned.1.call-update
  136.1 69.6 %all-reduce.5.cloned.1.call-done = (f32[64,704]{1,0:T(8,128)}, f32[64,704]{1,0:T(8,128)}) async-done(((f32[64,704]{1,0:T(8,128)}, f32[64,704]{1,0:T(8,128)}), (f32[64,704]{1,0:T(8,128)}, f32[64,704]{1,0:T(8,128)})) %all-reduce.5.cloned.1.call-update) | async-done | bytes 360464 | tf_op jit(solution)/shard_map/psum | solution.py:13
  205.7 1.2 fusion
  206.9 10.3 %psum.63 = f32[64,128]{1,0:T(8,128)S(1)} all-reduce(f32[64,128]{1,0:T(8,128)S(1)} %fusion), channel_id=1, replica_groups=mesh['ra'=8,'cb'=4] {'cb'}, use_global_device_ids=true, to_apply=%region_9.10 | all-reduce | flops 8192 | bytes 65536 | tf_op jit(solution)/shard_map/psum | solution.py:31
  217.2 0.6 fusion.18
  (13 shorter events, 0.0 us)
Async XLA Ops:
  6.5 24.0 %copy-start.3 = (bf16[64,128]{1,0:T(8,128)(2,1)S(1)}, bf16[64,128]{1,0:T(8,128)(2,1)}, u32[]{:S(2)}) copy-start(bf16[64,128]{1,0:T(8,128)(2,1)} %param.9) | copy-start | bytes 49156
  6.5 26.0 %copy-start = (f32[128,704]{0,1:T(8,128)S(1)}, f32[128,704]{0,1:T(8,128)}, u32[]{:S(2)}) copy-start(f32[128,704]{0,1:T(8,128)} %param.11) | copy-start | bytes 1081348
  6.5 96.3 %all-reduce.7.cloned.1.call-start = ((), (), s32[]{:S(2)}) async-start(), calls=%async_computation.1 | async-start | bytes 786432 | tf_op jit(solution)/shard_map/psum | solution.py:13
  30.6 1.9 copy-start.4
  32.5 70.4 %copy-start.6 = (f32[704,128]{1,0:T(8,128)S(1)}, f32[704,128]{1,0:T(8,128)}, u32[]{:S(2)}) copy-start(f32[704,128]{1,0:T(8,128)} %param.13) | copy-start | bytes 1081348
  33.5 172.2 %all-reduce.5.cloned.1.call-start = ((), (), s32[]{:S(2)}) async-start(), calls=%async_computation | async-start | bytes 786432 | tf_op jit(solution)/shard_map/psum | solution.py:13
  102.9 31.3 %copy-start.1 = (f32[128,704]{0,1:T(8,128)S(1)}, f32[128,704]{0,1:T(8,128)}, u32[]{:S(2)}) copy-start(f32[128,704]{0,1:T(8,128)} %param.16) | copy-start | bytes 1081348
  102.9 31.3 %copy-start.5 = (f32[128]{0:T(128)S(1)}, f32[128]{0:T(128)}, u32[]{:S(2)}) copy-start(f32[128]{0:T(128)} %param.14) | copy-start | bytes 1540
  104.1 31.0 %copy-start.2 = (f32[128,704]{0,1:T(8,128)S(1)}, f32[128,704]{0,1:T(8,128)}, u32[]{:S(2)}) copy-start(f32[128,704]{0,1:T(8,128)} %param.15) | copy-start | bytes 1081348
  135.1 70.5 %copy-start.7 = (f32[704,128]{1,0:T(8,128)S(1)}, f32[704,128]{1,0:T(8,128)}, u32[]{:S(2)}) copy-start(f32[704,128]{1,0:T(8,128)} %param.17) | copy-start | bytes 1081348
Sparse Core Ops, SparseCore 0:
  33.6 69.2 all-reduce.6
  136.2 69.4 all-reduce.4
where the time goes:
time: 225 us
  waiting for transfers between devices  139 us (62%)
  blocking collectives  63.3 us (28%)
  between operations  13.5 us (6%)
  matrix products  7.15 us (3%)
    psum x2, waiting for transfers between devices, hidden_of(): gate_sum, up_sum = lax.psum((gate_part, up_part), 'ra')  139 us
    psum x2, blocking collectives, whole_sublayer(): square_total = lax.psum(jnp.sum(as_float * as_float, axis=1), 'ra')  42.7 us
    psum x2, blocking collectives, whole_sublayer(): branch = lax.psum(branch_part, 'cb')  20.7 us
  transfers between devices with their start and end apart: 2, of which 2 were waited for; matrix products, arithmetic and copies ran while one was open for 0% of the time, Pallas kernels for 0%

commit v1 on v0

--- a/solution.py
+++ b/solution.py
@@ -28,7 +28,7 @@
     branch_part = jnp.dot(
         hidden, down_weight.astype(jnp.bfloat16), preferred_element_type=jnp.float32
     )
-    branch = lax.psum(branch_part, "cb")
+    branch = jnp.sum(lax.all_gather(branch_part, "cb"), axis=0)
     return (residual_weight * as_float + branch).astype(jnp.bfloat16)
 
 

time: 225 us -> 215 us (0.956)
  blocking collectives: 63.3 us -> 53.6 us
    psum x2 -> x0, blocking collectives: 20.7 us -> none  [whole_sublayer(): branch = lax.psum(branch_part, 'cb')]
    all_gather x0 -> x2, blocking collectives: none -> 11 us  [whole_sublayer(): branch = jnp.sum(lax.all_gather(branch_part, 'cb'), axis=0)]
where the time goes in v1:
time: 215 us
  waiting for transfers between devices  139 us (65%)
  blocking collectives  53.6 us (25%)
  between operations  13.5 us (6%)
  matrix products  7.1 us (3%)
    psum x2, waiting for transfers between devices, hidden_of(): gate_sum, up_sum = lax.psum((gate_part, up_part), 'ra')  139 us
    psum x2, blocking collectives, whole_sublayer(): square_total = lax.psum(jnp.sum(as_float * as_float, axis=1), 'ra')  42.7 us
    all_gather x2, blocking collectives, whole_sublayer(): branch = jnp.sum(lax.all_gather(branch_part, 'cb'), axis=0)  11 us
  transfers between devices with their start and end apart: 2, of which 2 were waited for; matrix products, arithmetic and copies ran while one was open for 0% of the time, Pallas kernels for 0%

profile of v1, /device:TPU:0, one launch (start us, length us, event | category | flops | bytes accessed | tf_op | source)
XLA Modules:
  0.0 214.7 jit_solution(11234577570022851380)
XLA Ops:
  6.5 0.0 all-reduce.7.cloned.1.call-start
  6.5 0.9 fusion.14
  7.4 23.1 %psum.42 = f32[64]{0:T(128)S(1)} all-reduce(f32[64]{0:T(128)S(1)} %fusion.14), channel_id=1, replica_groups=mesh['ra'=8,'cb'=4] {'ra'}, use_global_device_ids=true, to_apply=%region_1.0 | all-reduce | flops 64 | bytes 512 | tf_op jit(solution)/shard_map/psum | solution.py:25
  30.6 0.0 copy-start.4
  30.6 1.9 fusion.8
  32.5 0.0 copy-done
  32.5 0.9 fusion.10
  33.4 0.0 all-reduce.7.cloned.1.call-update
  33.5 0.0 all-reduce.5.cloned.1.call-start
  33.5 69.4 %all-reduce.7.cloned.1.call-done = (f32[64,704]{1,0:T(8,128)}, f32[64,704]{1,0:T(8,128)}) async-done(((f32[64,704]{1,0:T(8,128)}, f32[64,704]{1,0:T(8,128)}), (f32[64,704]{1,0:T(8,128)}, f32[64,704]{1,0:T(8,128)})) %all-reduce.7.cloned.1.call-update) | async-done | bytes 360464 | tf_op jit(solution)/shard_map/psum | solution.py:13
  102.9 1.2 fusion.6
  104.1 0.0 copy-start.1
  104.1 5.5 %all-gather = f32[256,128]{1,0:T(8,128)S(1)} all-gather(f32[64,128]{1,0:T(8,128)S(1)} %fusion.6), channel_id=2, replica_groups=mesh['ra'=8,'cb'=4] {'cb'}, dimensions={0}, use_global_device_ids=true | all-gather | bytes 163840 | tf_op jit(solution)/shard_map/all_gather | solution.py:31
  109.7 0.0 copy-start.2
  109.7 0.1 fusion.19
  109.8 19.5 %psum.45 = f32[64]{0:T(128)S(1)} all-reduce(f32[64]{0:T(128)S(1)} %get-tuple-element.9), channel_id=1, replica_groups=mesh['ra'=8,'cb'=4] {'ra'}, use_global_device_ids=true, to_apply=%region_6.7 | all-reduce | flops 64 | bytes 512 | tf_op jit(solution)/shard_map/psum | solution.py:25
  129.3 0.0 copy-done.1
  129.3 0.9 fusion.2
  130.3 0.9 fusion.4
  131.2 0.0 all-reduce.5.cloned.1.call-update
  131.2 69.3 %all-reduce.5.cloned.1.call-done = (f32[64,704]{1,0:T(8,128)}, f32[64,704]{1,0:T(8,128)}) async-done(((f32[64,704]{1,0:T(8,128)}, f32[64,704]{1,0:T(8,128)}), (f32[64,704]{1,0:T(8,128)}, f32[64,704]{1,0:T(8,128)})) %all-reduce.5.cloned.1.call-update) | async-done | bytes 360464 | tf_op jit(solution)/shard_map/psum | solution.py:13
  200.6 1.2 fusion
  201.8 5.4 %all-gather.1 = f32[256,128]{1,0:T(8,128)S(1)} all-gather(f32[64,128]{1,0:T(8,128)S(1)} %fusion), channel_id=3, replica_groups=mesh['ra'=8,'cb'=4] {'cb'}, dimensions={0}, use_global_device_ids=true | all-gather | bytes 163840 | tf_op jit(solution)/shard_map/all_gather | solution.py:31
  207.2 0.6 fusion.18
  (15 shorter events, 0.1 us)
Async XLA Ops:
  6.5 24.0 %copy-start.3 = (bf16[64,128]{1,0:T(8,128)(2,1)S(1)}, bf16[64,128]{1,0:T(8,128)(2,1)}, u32[]{:S(2)}) copy-start(bf16[64,128]{1,0:T(8,128)(2,1)} %param.9) | copy-start | bytes 49156
  6.5 26.0 %copy-start = (f32[128,704]{0,1:T(8,128)S(1)}, f32[128,704]{0,1:T(8,128)}, u32[]{:S(2)}) copy-start(f32[128,704]{0,1:T(8,128)} %param.11) | copy-start | bytes 1081348
  6.5 96.3 %all-reduce.7.cloned.1.call-start = ((), (), s32[]{:S(2)}) async-start(), calls=%async_computation.1 | async-start | bytes 786432 | tf_op jit(solution)/shard_map/psum | solution.py:13
  30.6 1.9 copy-start.4
  32.5 70.4 %copy-start.6 = (f32[704,128]{1,0:T(8,128)S(1)}, f32[704,128]{1,0:T(8,128)}, u32[]{:S(2)}) copy-start(f32[704,128]{1,0:T(8,128)} %param.13) | copy-start | bytes 1081348
  33.5 167.1 %all-reduce.5.cloned.1.call-start = ((), (), s32[]{:S(2)}) async-start(), calls=%async_computation | async-start | bytes 786432 | tf_op jit(solution)/shard_map/psum | solution.py:13
  104.1 25.2 %copy-start.1 = (f32[128,704]{0,1:T(8,128)S(1)}, f32[128,704]{0,1:T(8,128)}, u32[]{:S(2)}) copy-start(f32[128,704]{0,1:T(8,128)} %param.16) | copy-start | bytes 1081348
  109.7 19.7 %copy-start.5 = (f32[128]{0:T(128)S(1)}, f32[128]{0:T(128)}, u32[]{:S(2)}) copy-start(f32[128]{0:T(128)} %param.14) | copy-start | bytes 1540
  109.7 20.6 %copy-start.2 = (f32[128,704]{0,1:T(8,128)S(1)}, f32[128,704]{0,1:T(8,128)}, u32[]{:S(2)}) copy-start(f32[128,704]{0,1:T(8,128)} %param.15) | copy-start | bytes 1081348
  130.3 70.3 %copy-start.7 = (f32[704,128]{1,0:T(8,128)S(1)}, f32[704,128]{1,0:T(8,128)}, u32[]{:S(2)}) copy-start(f32[704,128]{1,0:T(8,128)} %param.17) | copy-start | bytes 1081348
Sparse Core Ops, SparseCore 0:
  33.6 69.2 all-reduce.6
  131.3 69.1 all-reduce.4
